TPU v7x, 32 devices: a whole 2x2x4 slice. The times are simulated.
32 devices in a mesh: ep: 8 (over z, x), tp: 4 (over y, core).
Axes of the slice: x: 2, y: 2, z: 4, core: 2. Of those that a mesh axis runs over, the one named last changes fastest.
Arguments:
- queries: bfloat16 [12288, 1024], P(('ep', 'tp')), may hold values from -250 to 250
- keys_values: bfloat16 [2, 12288, 256], P(None, ('ep', 'tp')), may hold values from -8 to 8
- sink_logits: float32 [16], replicated, may hold values from 2 to 6
- moe_rows: bfloat16 [2048, 2048], P('ep'), may hold values from -600 to 600
- norm_gain: float32 [2048], replicated, may hold values from 0.1 to 1.9
- group_choice: int32 [2048], P('ep'), may hold values from 0 to 1, as said below
- member_choice: int32 [2048, 2], P('ep'), may hold values from 0 to 3, as said below
- route_weight: float32 [2048, 2], P('ep'), may hold values from 0.1 to 1
- w_gate: bfloat16 [8, 2048, 2048], P('ep', None, 'tp'), may hold values from -0.125 to 0.125
- w_up: bfloat16 [8, 2048, 2048], P('ep', None, 'tp'), may hold values from -0.125 to 0.125
- w_down: bfloat16 [8, 2048, 2048], P('ep', None, 'tp'), may hold values from -0.125 to 0.125
Outputs:
- attended: bfloat16 [12288, 1024], P(('ep', 'tp'))
- mixed: bfloat16 [2048, 2048], P('ep', 'tp')
Inputs may be any that keep to these rules, and one draw needn't show every extreme that they name: With expert = group_choice * 4 + member_choice, within the 256 rows of one index of ep no expert is named by more than 128 rows, and some expert is named by exactly 128 rows. `member_choice`: the 2 entries of a row differ.
All inputs are finite; a program needn't handle non-finite values.
Results may differ from a plain program's by a relative error of at most 0.007.
Values may be sent and summed in bfloat16 or wider, within the bound.
A program may use at most 64 MiB of HBM per device.

v0:
```python
import functools

import jax
import jax.numpy as jnp
from jax import lax
from jax.experimental import pallas as pl
from jax.experimental.pallas import tpu as pltpu
from jax.sharding import PartitionSpec as P

QH = 16
KVH = 4
HD = 64
WINDOW = 128
EPG = 4
TOP = 2
CORES = 2
MESH = pl.DeviceIdType.MESH
F32 = jnp.float32
BF16 = jnp.bfloat16


def flipped(e, d, n):
    d = lax.rem(n - d, n)
    out = 0
    bit = 1
    while bit < n:
        out = out + bit * lax.rem(e // bit + d // bit, 2)
        bit *= 2
    return out


def kernel(
    n, tp, cap,
    q_ref, kv_ref, sink_ref, rows_ref, gain_ref, group_ref, member_ref, rw_ref,
    wg_hbm, wu_hbm, wd_hbm,
    att_ref, mix_ref,
    wg, wu, wd, kvj, nrm, posm, S, X, H, O, R, acc, line, col,
    loc, edge_s, edge_r, s_s, r1, x_s, x2, x3, h_s, h2, h3, o_s, o_r,
):
    e = lax.axis_index("ep")
    t = lax.axis_index("tp")
    ny = tp // CORES
    y = t // CORES
    core = lax.rem(t, CORES)
    mate = y * CORES + (1 - core)
    tokens, width = rows_ref.shape
    dc = width // tp
    ffs = wg.shape[1]
    length = q_ref.shape[0]
    lin = e * tp + t
    total = n * tp
    after = lax.rem(lin + 1, total)
    before = lax.rem(lin + total - 1, total)

    loads = [
        pltpu.make_async_copy(wg_hbm.at[0], wg, loc.at[0]),
        pltpu.make_async_copy(wu_hbm.at[0], wu, loc.at[1]),
        pltpu.make_async_copy(wd_hbm.at[0], wd, loc.at[2]),
        pltpu.make_async_copy(kv_ref, kvj.at[:, pl.ds(WINDOW, length)], loc.at[3]),
    ]
    for c in loads:
        c.start()

    def ypeer(j):
        return lax.rem(y + j, ny) * CORES + core

    barrier = pltpu.get_barrier_semaphore()

    def greet(d, _):
        pl.semaphore_signal(barrier, inc=1, device_id=(flipped(e, d, n), t), device_id_type=MESH)
        return 0

    lax.fori_loop(1, n, greet, 0)
    for j in range(1, ny):
        pl.semaphore_signal(barrier, inc=1, device_id=(e, ypeer(j)), device_id_type=MESH)
    pl.semaphore_signal(barrier, inc=1, device_id=(e, mate), device_id_type=MESH)
    for lin2 in (after, before):
        pl.semaphore_signal(
            barrier, inc=1, device_id=(lin2 // tp, lax.rem(lin2, tp)), device_id_type=MESH
        )

    chunk = 32

    def norm_rows(r, _):
        at = pl.ds(pl.multiple_of(r * chunk, chunk), chunk)
        v = rows_ref[at, :].astype(F32)
        m = jnp.mean(v * v, axis=1, keepdims=True)
        nv = (v * lax.rsqrt(m + 1e-06) * gain_ref[...]).astype(BF16)
        for k in range(tp):
            nrm[k, at, :] = nv[:, k * dc : (k + 1) * dc]
        return 0

    lax.fori_loop(0, tokens // chunk, norm_rows, 0)

    a_i = lax.broadcasted_iota(jnp.int32, (tokens, tokens), 0)
    b_i = lax.broadcasted_iota(jnp.int32, (tokens, tokens), 1)
    erow = lax.broadcasted_iota(jnp.int32, (n, tokens), 0)
    e0 = group_ref[...] * EPG + member_ref[0:1, :]
    e1 = group_ref[...] * EPG + member_ref[1:2, :]
    named = (e0 == erow) | (e1 == erow)
    upper = (a_i < b_i).astype(F32).astype(BF16)
    pos = jnp.dot(named.astype(F32).astype(BF16), upper, preferred_element_type=F32)
    posm[...] = jnp.where(named, pos, -1.0).astype(jnp.int32)
    line[0:1, :] = e0.astype(F32)
    line[1:2, :] = e1.astype(F32)
    line[2:3, :] = jnp.sum(jnp.where(e0 == erow, pos, 0.0), axis=0, keepdims=True)
    line[3:4, :] = jnp.sum(jnp.where(e1 == erow, pos, 0.0), axis=0, keepdims=True)
    line[4:6, :] = rw_ref[...]
    line[6:, :] = jnp.zeros((122, tokens), F32)
    col[...] = line[...].T

    def slots_of(x):
        slot = lax.broadcasted_iota(jnp.int32, (cap, tokens), 0)
        return (posm[pl.ds(x, 1), :] == slot).astype(F32).astype(BF16)

    def build(d, _):
        S[d] = jnp.dot(slots_of(flipped(e, d, n)), nrm[t], preferred_element_type=F32).astype(BF16)
        return 0

    lax.fori_loop(1, n, build, 0)
    mine = slots_of(e)
    for k in range(tp):
        X[0, k] = jnp.dot(mine, nrm[k], preferred_element_type=F32).astype(BF16)

    loads[3].wait()
    pl.semaphore_wait(barrier, (n - 1) + (ny - 1) + 1 + 2)

    def dispatch(d, _):
        pltpu.make_async_remote_copy(
            src_ref=S.at[d], dst_ref=X.at[d, t], send_sem=s_s.at[d], recv_sem=r1.at[d],
            device_id=(flipped(e, d, n), t), device_id_type=MESH,
        ).start()
        return 0

    lax.fori_loop(1, n, dispatch, 0)
    edge = pltpu.make_async_remote_copy(
        src_ref=kvj.at[:, pl.ds(length, WINDOW)], dst_ref=kvj.at[:, pl.ds(0, WINDOW)],
        send_sem=edge_s, recv_sem=edge_r,
        device_id=(after // tp, lax.rem(after, tp)), device_id_type=MESH,
    )
    edge.start()

    def expect(ref, sem):
        pltpu.make_async_copy(ref, ref, sem).wait()

    def spread(buf, d, sends, to_y, to_mate):
        for j in range(1, ny):
            pltpu.make_async_remote_copy(
                src_ref=buf.at[d, t], dst_ref=buf.at[d, t], send_sem=sends.at[d],
                recv_sem=to_y.at[d], device_id=(e, ypeer(j)), device_id_type=MESH,
            ).start()
        pltpu.make_async_remote_copy(
            src_ref=buf.at[d, t], dst_ref=buf.at[d, t], send_sem=sends.at[d],
            recv_sem=to_mate.at[d], device_id=(e, mate), device_id_type=MESH,
        ).start()

    def relay(buf, d, sends, to_y, to_mate):
        expect(buf.at[d, pl.ds(0, ny - 1)], to_y.at[d])
        for j in range(1, ny):
            k = ypeer(j)
            pltpu.make_async_remote_copy(
                src_ref=buf.at[d, k], dst_ref=buf.at[d, k], send_sem=sends.at[d],
                recv_sem=to_mate.at[d], device_id=(e, mate), device_id_type=MESH,
            ).start()

    def forward(d):
        expect(X.at[d, t], r1.at[d])
        spread(X, d, x_s, x2, x3)

    def gate_up(d):
        x = jnp.concatenate([X[d, k] for k in range(tp)], axis=1)
        step = min(256, ffs)
        for c in range(0, ffs, step):
            g = jnp.dot(x, wg[:, c : c + step], preferred_element_type=F32)
            u = jnp.dot(x, wu[:, c : c + step], preferred_element_type=F32)
            H[d, t, :, c : c + step] = (g / (1.0 + jnp.exp(-g)) * u).astype(BF16)

    def down(d):
        h = jnp.concatenate([H[d, k] for k in range(tp)], axis=1)
        O[d] = jnp.dot(h, wd[...], preferred_element_type=F32).astype(BF16)

    def combine(d, ref):
        x = flipped(e, d, n)
        first = col[:, 0:1] == x.astype(F32)
        second = col[:, 1:2] == x.astype(F32)
        where = jnp.where(first, col[:, 2:3], jnp.where(second, col[:, 3:4], -1.0))
        weight = jnp.where(first, col[:, 4:5], jnp.where(second, col[:, 5:6], 0.0))
        slot = lax.broadcasted_iota(jnp.int32, (tokens, cap), 1).astype(F32)
        pick = (where == slot).astype(F32).astype(BF16)
        acc[...] += weight * jnp.dot(pick, ref[d], preferred_element_type=F32)

    sharing = QH // KVH

    def attend(b, half):
        base = pl.multiple_of(b * WINDOW, WINDOW)
        qi = lax.broadcasted_iota(jnp.int32, (WINDOW, 2 * WINDOW), 0)
        kj = lax.broadcasted_iota(jnp.int32, (WINDOW, 2 * WINDOW), 1)
        dist = qi + WINDOW - kj
        seen = (dist >= 0) & (dist < WINDOW) & (lin * length + base + kj - WINDOW >= 0)
        for pair in range(half * QH // 4, (half + 1) * QH // 4):
            h = 2 * pair // sharing
            lo = (h // 2) * 128
            keys = kvj[0, pl.ds(base, 2 * WINDOW), lo : lo + 128]
            vals = kvj[1, pl.ds(base, 2 * WINDOW), lo : lo + 128]
            off = (h % 2) * HD
            keys = keys[:, off : off + HD]
            vals = vals[:, off : off + HD]
            qp = q_ref[pl.ds(base, WINDOW), pair * 128 : (pair + 1) * 128]
            outs = []
            for g in range(2):
                s = lax.dot_general(
                    qp[:, g * HD : (g + 1) * HD], keys, (((1,), (1,)), ((), ())),
                    preferred_element_type=F32,
                ) * HD ** (-0.5)
                s = jnp.where(seen, s, -1e30)
                sink = sink_ref[2 * pair + g]
                top = jnp.maximum(jnp.max(s, axis=1, keepdims=True), sink)
                w = jnp.exp(s - top)
                tot = jnp.sum(w, axis=1, keepdims=True) + jnp.exp(sink - top)
                o = jnp.dot(w.astype(BF16), vals, preferred_element_type=F32)
                outs.append((o / tot).astype(BF16))
            att_ref[pl.ds(base, WINDOW), pair * 128 : (pair + 1) * 128] = jnp.concatenate(outs, axis=1)

    acc[...] = jnp.zeros_like(acc)
    loads[0].wait()
    loads[1].wait()
    units = 2 * (length // WINDOW)

    def step(i, _):
        @pl.when(i < n)
        def _():
            @pl.when(i > 0)
            def _():
                expect(X.at[i, pl.ds(0, ny)], x3.at[i])
            gate_up(i)
            spread(H, i, h_s, h2, h3)

        @pl.when(i == 0)
        def _():
            forward(1)

        @pl.when(i + 2 < n)
        def _():
            forward(i + 2)

        @pl.when(i == 0)
        def _():
            edge.wait()
            loads[2].wait()

        for half in range(2):
            @pl.when((i < units) & (lax.rem(i, 2) == half))
            def _(half=half):
                attend(i // 2, half)

        @pl.when(i + 1 < n)
        def _():
            relay(X, i + 1, x_s, x2, x3)

        @pl.when((i >= 1) & (i - 1 < n))
        def _():
            relay(H, i - 1, h_s, h2, h3)

        @pl.when((i >= 2) & (i - 2 < n))
        def _():
            d = i - 2
            expect(H.at[d, pl.ds(0, ny)], h3.at[d])
            down(d)

            @pl.when(d > 0)
            def _():
                pltpu.make_async_remote_copy(
                    src_ref=O.at[d], dst_ref=R.at[d], send_sem=o_s.at[d], recv_sem=o_r.at[d],
                    device_id=(flipped(e, d, n), t), device_id_type=MESH,
                ).start()

            @pl.when(d == 0)
            def _():
                combine(d, O)

        @pl.when(i >= 5)
        def _():
            d = i - 4
            expect(R.at[d], o_r.at[d])
            combine(d, R)

        return 0

    lax.fori_loop(0, n + 4, step, 0)
    mix_ref[...] = acc[...].astype(BF16)

    def drain(d, _):
        @pl.when(d > 0)
        def _():
            expect(S.at[d], s_s.at[d])
            expect(X.at[d, pl.ds(0, 2 * ny - 1)], x_s.at[d])
            expect(O.at[d], o_s.at[d])
        expect(H.at[d, pl.ds(0, 2 * ny - 1)], h_s.at[d])
        return 0

    lax.fori_loop(0, n, drain, 0)


def shards(
    queries, keys_values, sink_logits, moe_rows, norm_gain, group_choice, member_choice,
    route_weight, w_gate, w_up, w_down,
):
    n = lax.axis_size("ep")
    tp = lax.axis_size("tp")
    assert w_gate.shape[0] == 1
    tokens, width = moe_rows.shape
    cap = 2 * TOP * tokens // n
    ffs = w_gate.shape[2]
    out = w_down.shape[2]
    ff = w_down.shape[1]
    length = queries.shape[0]
    vmem = pl.BlockSpec(memory_space=pltpu.VMEM)
    anyspace = pl.BlockSpec(memory_space=pl.ANY)
    dma = pltpu.SemaphoreType.DMA
    return pl.pallas_call(
        functools.partial(kernel, n, tp, cap),
        out_shape=(
            pltpu.VMEM(queries.shape, BF16),
            pltpu.VMEM((tokens, out), BF16),
        ),
        in_specs=[
            vmem, anyspace, pl.BlockSpec(memory_space=pltpu.SMEM), vmem, vmem, vmem, vmem, vmem,
            anyspace, anyspace, anyspace,
        ],
        out_specs=(vmem, vmem),
        scratch_shapes=[
            pltpu.VMEM((width, ffs), BF16),
            pltpu.VMEM((width, ffs), BF16),
            pltpu.VMEM((ff, out), BF16),
            pltpu.VMEM((2, WINDOW + length, keys_values.shape[2]), BF16),
            pltpu.VMEM((tp, tokens, width // tp), BF16),
            pltpu.VMEM((n, tokens), jnp.int32),
            pltpu.VMEM((n, cap, width // tp), BF16),
            pltpu.VMEM((n, tp, cap, width // tp), BF16),
            pltpu.VMEM((n, tp, cap, ffs), BF16),
            pltpu.VMEM((n, cap, out), BF16),
            pltpu.VMEM((n, cap, out), BF16),
            pltpu.VMEM((tokens, out), F32),
            pltpu.VMEM((128, tokens), F32),
            pltpu.VMEM((tokens, 128), F32),
            dma((4,)), dma, dma,
            dma((n,)), dma((n,)), dma((n,)), dma((n,)), dma((n,)),
            dma((n,)), dma((n,)), dma((n,)), dma((n,)), dma((n,)),
        ],
        compiler_params=pltpu.CompilerParams(
            collective_id=0, has_side_effects=True, vmem_limit_bytes=56 * 1024 * 1024
        ),
    )(
        queries, keys_values, sink_logits, moe_rows, norm_gain.reshape(1, width),
        group_choice.reshape(1, tokens), member_choice.T, route_weight.T, w_gate, w_up, w_down,
    )


def solution(mesh):
    in_specs = (
        P(("ep", "tp"), None),
        P(None, ("ep", "tp"), None),
        P(),
        P("ep", None),
        P(),
        P("ep"),
        P("ep", None),
        P("ep", None),
        P("ep", None, "tp"),
        P("ep", None, "tp"),
        P("ep", None, "tp"),
    )
    out_specs = (P(("ep", "tp"), None), P("ep", "tp"))
    return jax.shard_map(shards, mesh=mesh, in_specs=in_specs, out_specs=out_specs, check_vma=False)
```

profile of v0, /device:TPU:18, one launch (start us, length us, event | category | flops | bytes accessed | tf_op | source)
XLA Modules:
  0.0 81.1 jit_solution(2350827922239511094)
XLA Ops:
  0.6 78.9 %shard_map.122 = (bf16[384,1024]{1,0:T(8,128)(2,1)S(1)}, bf16[256,512]{1,0:T(8,128)(2,1)S(1)}) custom-call(bf16[384,1024]{1,0:T(8,128)(2,1)} %q_ref.1, bf16[2,384,256]{2,1,0:T(8,128)(2,1)} %kv_ref.1, f32[16]{0:T(128)} %sink_ref.1, bf16[256,2048]{1,0:T(8,128)(2,1)} %rows_ref.1, f32[1,2048]{1,0:T(1,128)} %bitcast.4, s32[1,256]{1,0:T(1,128)} %bitcast.7, ...), custom_call_target="tpu_custom_call" | custom-call | tf_op jit(solution)/shard_map/pallas_call | solution.py:320
  79.5 0.9 %copy.15 = bf16[384,1024]{1,0:T(8,128)(2,1)} copy(bf16[384,1024]{1,0:T(8,128)(2,1)S(1)} %get-tuple-element.2) | data formatting | bytes 1572864
  80.4 0.7 copy.16
where the time goes:
time: 81.2 us; the launch traced here: 81.1 us
  Pallas kernels  78.9 us (97%)
  local copies, waits for them, and re-layouts  1.58 us (2%)
    pallas_call x1, Pallas kernels, shards(): pl.pallas_call(functools.partial(kernel, n, tp, cap), out_shape=(pltpu.VM...  78.9 us

commit v1 on v0

v1 whole, which is shorter than its diff:
```python
import functools

import jax
import jax.numpy as jnp
from jax import lax
from jax.experimental import pallas as pl
from jax.experimental.pallas import tpu as pltpu
from jax.sharding import PartitionSpec as P

QH = 16
KVH = 4
HD = 64
WINDOW = 128
EPG = 4
TOP = 2
CORES = 2
WIDE = 4
RAWAT = 2
LAG = 6
MESH = pl.DeviceIdType.MESH
F32 = jnp.float32
BF16 = jnp.bfloat16


def kernel(
    n, tp, cap,
    q_hbm, kv_hbm, sink_ref, rows_hbm, gain_ref, group_ref, member_ref, rw_ref,
    wg_hbm, wu_hbm, wd_hbm,
    att_ref, mix_ref,
    wg, wu, wd, q, rows, kvj, nrm, raw, posm, S, SN, X, H, O, R, acc, line, col,
    loc, edge_s, edge_r, raw_s, raw_r, pos_s, pos_r, s_s, r1, x_s, x2, x3, h_s, h2, h3, o_s, o_r,
):
    e = lax.axis_index("ep")
    t = lax.axis_index("tp")
    ny = tp // CORES
    y = t // CORES
    core = lax.rem(t, CORES)
    mate = y * CORES + (1 - core)
    near = min(EPG, n)
    sides = n // near
    wide = min(WIDE, near)
    tokens, width = rows.shape
    dc = width // tp
    ffs = wg.shape[1]
    length = q.shape[0]
    lin = e * tp + t
    total = n * tp
    after = lax.rem(lin + 1, total)
    before = lax.rem(lin + total - 1, total)
    home = core * ny
    own = home + y

    def block_of(k):
        return (k % CORES) * ny + k // CORES

    def partner(m):
        out = 0
        bit = 1
        while bit < n:
            out = out + bit * lax.rem(e // bit + m // bit, 2)
            bit *= 2
        return out

    def ypeer(j):
        return lax.rem(y + j, ny) * CORES + core

    barrier = pltpu.get_barrier_semaphore()

    def greet(m, _):
        pl.semaphore_signal(barrier, inc=1, device_id=(partner(m), t), device_id_type=MESH)
        return 0

    lax.fori_loop(1, n, greet, 0)
    for j in range(1, ny):
        pl.semaphore_signal(barrier, inc=1, device_id=(e, ypeer(j)), device_id_type=MESH)
    pl.semaphore_signal(barrier, inc=1, device_id=(e, mate), device_id_type=MESH)
    for lin2 in (after, before):
        pl.semaphore_signal(
            barrier, inc=1, device_id=(lin2 // tp, lax.rem(lin2, tp)), device_id_type=MESH
        )

    loads = [
        pltpu.make_async_copy(rows_hbm, rows, loc.at[0]),
        pltpu.make_async_copy(wg_hbm.at[0], wg, loc.at[1]),
        pltpu.make_async_copy(wu_hbm.at[0], wu, loc.at[2]),
        pltpu.make_async_copy(q_hbm, q, loc.at[3]),
        pltpu.make_async_copy(kv_hbm, kvj.at[:, pl.ds(WINDOW, length)], loc.at[4]),
        pltpu.make_async_copy(wd_hbm.at[0], wd, loc.at[5]),
    ]
    loads[0].start()

    a_i = lax.broadcasted_iota(jnp.int32, (tokens, tokens), 0)
    b_i = lax.broadcasted_iota(jnp.int32, (tokens, tokens), 1)
    erow = lax.broadcasted_iota(jnp.int32, (n, tokens), 0)
    e0 = group_ref[...] * EPG + member_ref[0:1, :]
    e1 = group_ref[...] * EPG + member_ref[1:2, :]
    named = (e0 == erow) | (e1 == erow)
    upper = (a_i < b_i).astype(F32).astype(BF16)
    pos = jnp.dot(named.astype(F32).astype(BF16), upper, preferred_element_type=F32)
    posm[0] = jnp.where(named, pos, -1.0).astype(jnp.int32)
    line[0:1, :] = e0.astype(F32)
    line[1:2, :] = e1.astype(F32)
    line[2:3, :] = jnp.sum(jnp.where(e0 == erow, pos, 0.0), axis=0, keepdims=True)
    line[3:4, :] = jnp.sum(jnp.where(e1 == erow, pos, 0.0), axis=0, keepdims=True)
    line[4:6, :] = rw_ref[...]
    line[6:, :] = jnp.zeros((122, tokens), F32)
    col[...] = line[...].T
    acc[...] = jnp.zeros_like(acc)

    @pl.when(lin == 0)
    def _():
        kvj[:, 0:WINDOW, :] = jnp.zeros((2, WINDOW, kvj.shape[2]), BF16)

    chunk = 32

    def norm_rows(r, _):
        at = pl.ds(pl.multiple_of(r * chunk, chunk), chunk)
        v = rows[at, :].astype(F32)
        m = jnp.mean(v * v, axis=1, keepdims=True)
        nv = (v * lax.rsqrt(m + 1e-06) * gain_ref[...]).astype(BF16)
        for k in range(tp):
            nrm[block_of(k), at, :] = nv[:, k * dc : (k + 1) * dc]
        return 0

    loads[0].wait()
    for c in loads[1:]:
        c.start()
    with jax.named_scope("norm"):
        lax.fori_loop(0, tokens // chunk, norm_rows, 0)

    def slots_of(side, x):
        slot = lax.broadcasted_iota(jnp.int32, (cap, tokens), 0)
        return (posm[side, pl.ds(x, 1), :] == slot).astype(F32).astype(BF16)

    def gathered(slots, rows_of):
        return jnp.dot(slots, rows_of, preferred_element_type=F32).astype(BF16)

    edge = pltpu.make_async_remote_copy(
        src_ref=kv_hbm.at[:, pl.ds(length - WINDOW, WINDOW)], dst_ref=kvj.at[:, pl.ds(0, WINDOW)],
        send_sem=edge_s, recv_sem=edge_r,
        device_id=(after // tp, lax.rem(after, tp)), device_id_type=MESH,
    )

    def send_rows(m):
        pltpu.make_async_remote_copy(
            src_ref=S.at[m], dst_ref=X.at[m, own], send_sem=s_s.at[m], recv_sem=r1.at[m],
            device_id=(partner(lax.rem(m, near)), t), device_id_type=MESH,
        ).start()

    def send_near(m):
        slots = slots_of(0, partner(m))
        if m < wide:
            for j in range(ny):
                SN[m, j] = gathered(slots, nrm[home + j])
            pltpu.make_async_remote_copy(
                src_ref=SN.at[m], dst_ref=X.at[m, pl.ds(home, ny)], send_sem=s_s.at[m],
                recv_sem=r1.at[m], device_id=(partner(m), t), device_id_type=MESH,
            ).start()
        else:
            S[m] = gathered(slots, nrm[own])
            send_rows(m)

    def send_raw(g, _):
        to = (partner(g * near), t)
        pltpu.make_async_remote_copy(
            src_ref=posm.at[0], dst_ref=posm.at[g], send_sem=pos_s.at[g], recv_sem=pos_r.at[g],
            device_id=to, device_id_type=MESH,
        ).start()
        pltpu.make_async_remote_copy(
            src_ref=nrm.at[own], dst_ref=raw.at[g], send_sem=raw_s.at[g], recv_sem=raw_r.at[g],
            device_id=to, device_id_type=MESH,
        ).start()
        return 0

    with jax.named_scope("barrier"):
        pl.semaphore_wait(barrier, (n - 1) + (ny - 1) + 1 + 2)
    with jax.named_scope("build"):
        first_near = near // 2
        send_near(first_near)
        lax.fori_loop(1, sides, send_raw, 0)
        for m in range(1, near - 1):
            if m != first_near:
                send_near(m)

    @pl.when(lin < total - 1)
    def _():
        edge.start()

    mine = slots_of(0, e)
    for k in range(tp):
        X[0, k] = gathered(mine, nrm[k])

    def expect(ref, sem):
        pltpu.make_async_copy(ref, ref, sem).wait()

    def spread(buf, m, sends, to_y):
        for j in range(1, ny):
            pltpu.make_async_remote_copy(
                src_ref=buf.at[m, own], dst_ref=buf.at[m, own], send_sem=sends.at[m],
                recv_sem=to_y.at[m], device_id=(e, ypeer(j)), device_id_type=MESH,
            ).start()

    def relay(buf, m, sends, to_mate):
        half = buf.at[m, pl.ds(home, ny)]
        pltpu.make_async_remote_copy(
            src_ref=half, dst_ref=half, send_sem=sends.at[m],
            recv_sem=to_mate.at[m], device_id=(e, mate), device_id_type=MESH,
        ).start()

    def gate_up(m):
        x = jnp.concatenate([X[m, block_of(k)] for k in range(tp)], axis=1)
        step = min(256, ffs)
        for c in range(0, ffs, step):
            g = jnp.dot(x, wg[:, c : c + step], preferred_element_type=F32)
            u = jnp.dot(x, wu[:, c : c + step], preferred_element_type=F32)
            H[m, own, :, c : c + step] = (g / (1.0 + jnp.exp(-g)) * u).astype(BF16)

    def down(m):
        h = jnp.concatenate([H[m, block_of(k)] for k in range(tp)], axis=1)
        O[m] = jnp.dot(h, wd[...], preferred_element_type=F32).astype(BF16)

    def combine(m, ref):
        x = partner(m)
        first = col[:, 0:1] == x.astype(F32)
        second = col[:, 1:2] == x.astype(F32)
        where = jnp.where(first, col[:, 2:3], jnp.where(second, col[:, 3:4], -1.0))
        weight = jnp.where(first, col[:, 4:5], jnp.where(second, col[:, 5:6], 0.0))
        slot = lax.broadcasted_iota(jnp.int32, (tokens, cap), 1).astype(F32)
        pick = (where == slot).astype(F32).astype(BF16)
        acc[...] += weight * jnp.dot(pick, ref[m], preferred_element_type=F32)

    sharing = QH // KVH

    def attend(b, half):
        base = pl.multiple_of(b * WINDOW, WINDOW)
        qi = lax.broadcasted_iota(jnp.int32, (WINDOW, 2 * WINDOW), 0)
        kj = lax.broadcasted_iota(jnp.int32, (WINDOW, 2 * WINDOW), 1)
        dist = qi + WINDOW - kj
        seen = (dist >= 0) & (dist < WINDOW) & (lin * length + base + kj - WINDOW >= 0)
        for pair in range(half * QH // 4, (half + 1) * QH // 4):
            h = 2 * pair // sharing
            lo = (h // 2) * 128
            keys = kvj[0, pl.ds(base, 2 * WINDOW), lo : lo + 128]
            vals = kvj[1, pl.ds(base, 2 * WINDOW), lo : lo + 128]
            off = (h % 2) * HD
            keys = keys[:, off : off + HD]
            vals = vals[:, off : off + HD]
            qp = q[pl.ds(base, WINDOW), pair * 128 : (pair + 1) * 128]
            outs = []
            for g in range(2):
                s = lax.dot_general(
                    qp[:, g * HD : (g + 1) * HD], keys, (((1,), (1,)), ((), ())),
                    preferred_element_type=F32,
                ) * HD ** (-0.5)
                s = jnp.where(seen, s, -1e30)
                sink = sink_ref[2 * pair + g]
                top = jnp.maximum(jnp.max(s, axis=1, keepdims=True), sink)
                w = jnp.exp(s - top)
                tot = jnp.sum(w, axis=1, keepdims=True) + jnp.exp(sink - top)
                o = jnp.dot(w.astype(BF16), vals, preferred_element_type=F32)
                outs.append((o / tot).astype(BF16))
            att_ref[pl.ds(base, WINDOW), pair * 128 : (pair + 1) * 128] = jnp.concatenate(outs, axis=1)

    order = [0, *range(1, near - 1), *range(near, n), near - 1]

    def chosen(i):
        m = order[0]
        for j in range(1, n):
            m = jnp.where(i >= j, order[j], m)
        return m

    blocks = length // WINDOW
    units = 2 * blocks

    def take_raw(g):
        m = g * near
        with jax.named_scope("w_raw"):
            expect(posm.at[g], pos_r.at[g])
            expect(raw.at[g], raw_r.at[g])
        with jax.named_scope("relay_rows"):
            for r in range(1, near):
                S[m + r] = gathered(slots_of(g, partner(r)), raw[g])
                send_rows(m + r)
            X[m, own] = gathered(slots_of(g, e), raw[g])
            spread(X, m, x_s, x2)

    def take(i):
        m = chosen(i)

        @pl.when((i < n) & (m >= wide) & (lax.rem(m, near) != 0))
        def _():
            with jax.named_scope("w_r1"):
                expect(X.at[m, own], r1.at[m])
            spread(X, m, x_s, x2)

    def fill(i):
        m = chosen(i)

        @pl.when((i < n) & (m >= wide))
        def _():
            with jax.named_scope("w_x2"):
                expect(X.at[m, pl.ds(0, ny - 1)], x2.at[m])
            relay(X, m, x_s, x3)

        @pl.when((i < n) & (m < wide))
        def _():
            with jax.named_scope("w_r1n"):
                expect(X.at[m, pl.ds(0, ny)], r1.at[m])
            relay(X, m, x_s, x3)

    loads[1].wait()
    loads[2].wait()

    def when_raw(i, mark):
        for g in range(1, sides):
            @pl.when(i == near * (g - 1) + mark)
            def _(g=g):
                take_raw(g)

    early = lax.rem(e // (near // 2), 2) == lax.rem(e // near, 2)

    def step(i, _):
        @pl.when(early)
        def _():
            when_raw(i, RAWAT)

        @pl.when(i >= 3)
        def _():
            take(i + 1)

        @pl.when(i > 0)
        def _():
            fill(i)

        @pl.when((i >= 3) & (i < 3))
        def _():
            take(i + 1)

        @pl.when(i < n)
        def _():
            m = chosen(i)

            @pl.when(i > 0)
            def _():
                with jax.named_scope("w_x3"):
                    expect(X.at[m, pl.ds(0, ny)], x3.at[m])

            with jax.named_scope("gate_up"):
                gate_up(m)
            spread(H, m, h_s, h2)

        @pl.when(i < 3)
        def _():
            take(i + 1)

        @pl.when(i == 0)
        def _():
            loads[3].wait()
            loads[4].wait()
            loads[5].wait()

        @pl.when(i == units - 2)
        def _():
            @pl.when(lin > 0)
            def _():
                with jax.named_scope("w_edge"):
                    edge.wait_recv()

        @pl.when(jnp.logical_not(early))
        def _():
            when_raw(i, RAWAT)

        @pl.when((i >= 1) & (i - 1 < n))
        def _():
            m = chosen(i - 1)
            with jax.named_scope("w_h2"):
                expect(H.at[m, pl.ds(0, ny - 1)], h2.at[m])
            relay(H, m, h_s, h3)

        for half in range(2):
            @pl.when((i < units) & (lax.rem(i, 2) == half))
            def _(half=half):
                with jax.named_scope("attend"):
                    attend(blocks - 1 - i // 2, half)

        @pl.when((i >= 1) & (i - 1 < n))
        def _():
            m = chosen(i - 1)
            with jax.named_scope("w_h3"):
                expect(H.at[m, pl.ds(0, ny)], h3.at[m])
            with jax.named_scope("down"):
                down(m)

            @pl.when(i > 1)
            def _():
                pltpu.make_async_remote_copy(
                    src_ref=O.at[m], dst_ref=R.at[m], send_sem=o_s.at[m], recv_sem=o_r.at[m],
                    device_id=(partner(m), t), device_id_type=MESH,
                ).start()

            @pl.when(i == 1)
            def _():
                combine(m, O)

        @pl.when(i == 3)
        def _():
            send_near(near - 1)

        @pl.when((i > LAG) & (i - LAG < n))
        def _():
            m = chosen(i - LAG)
            with jax.named_scope("w_o"):
                expect(R.at[m], o_r.at[m])
            with jax.named_scope("combine"):
                combine(m, R)

        return 0

    lax.fori_loop(0, n + LAG, step, 0)
    mix_ref[...] = acc[...].astype(BF16)

    def drain(m, _):
        @pl.when(m >= wide)
        def _():
            @pl.when(lax.rem(m, near) > 0)
            def _():
                expect(S.at[m], s_s.at[m])

            expect(X.at[m, pl.ds(0, 2 * ny - 1)], x_s.at[m])

        @pl.when((m > 0) & (m < wide))
        def _():
            expect(SN.at[m], s_s.at[m])
            expect(X.at[m, pl.ds(0, ny)], x_s.at[m])

        @pl.when(m > 0)
        def _():
            expect(O.at[m], o_s.at[m])

        @pl.when((m > 0) & (m < sides))
        def _():
            expect(posm.at[m], pos_s.at[m])
            expect(raw.at[m], raw_s.at[m])

        expect(H.at[m, pl.ds(0, 2 * ny - 1)], h_s.at[m])
        return 0

    with jax.named_scope("drain"):
        lax.fori_loop(0, n, drain, 0)

    @pl.when(lin < total - 1)
    def _():
        edge.wait_send()


def shards(
    queries, keys_values, sink_logits, moe_rows, norm_gain, group_choice, member_choice,
    route_weight, w_gate, w_up, w_down,
):
    n = lax.axis_size("ep")
    tp = lax.axis_size("tp")
    assert w_gate.shape[0] == 1
    tokens, width = moe_rows.shape
    cap = 2 * TOP * tokens // n
    ffs = w_gate.shape[2]
    out = w_down.shape[2]
    ff = w_down.shape[1]
    length = queries.shape[0]
    vmem = pl.BlockSpec(memory_space=pltpu.VMEM)
    anyspace = pl.BlockSpec(memory_space=pl.ANY)
    dma = pltpu.SemaphoreType.DMA
    return pl.pallas_call(
        functools.partial(kernel, n, tp, cap),
        out_shape=(
            pltpu.VMEM(queries.shape, BF16),
            pltpu.VMEM((tokens, out), BF16),
        ),
        in_specs=[
            anyspace, anyspace, pl.BlockSpec(memory_space=pltpu.SMEM), anyspace, vmem, vmem, vmem, vmem,
            anyspace, anyspace, anyspace,
        ],
        out_specs=(vmem, vmem),
        scratch_shapes=[
            pltpu.VMEM((width, ffs), BF16),
            pltpu.VMEM((width, ffs), BF16),
            pltpu.VMEM((ff, out), BF16),
            pltpu.VMEM(queries.shape, BF16),
            pltpu.VMEM(moe_rows.shape, BF16),
            pltpu.VMEM((2, WINDOW + length, keys_values.shape[2]), BF16),
            pltpu.VMEM((tp, tokens, width // tp), BF16),
            pltpu.VMEM((n // min(EPG, n), tokens, width // tp), BF16),
            pltpu.VMEM((n // min(EPG, n), n, tokens), jnp.int32),
            pltpu.VMEM((n, cap, width // tp), BF16),
            pltpu.VMEM((min(EPG, n), tp // CORES, cap, width // tp), BF16),
            pltpu.VMEM((n, tp, cap, width // tp), BF16),
            pltpu.VMEM((n, tp, cap, ffs), BF16),
            pltpu.VMEM((n, cap, out), BF16),
            pltpu.VMEM((n, cap, out), BF16),
            pltpu.VMEM((tokens, out), F32),
            pltpu.VMEM((128, tokens), F32),
            pltpu.VMEM((tokens, 128), F32),
            dma((6,)), dma, dma,
            dma((n // min(EPG, n),)), dma((n // min(EPG, n),)), dma((n // min(EPG, n),)), dma((n // min(EPG, n),)),
            dma((n,)), dma((n,)), dma((n,)), dma((n,)), dma((n,)),
            dma((n,)), dma((n,)), dma((n,)), dma((n,)), dma((n,)),
        ],
        compiler_params=pltpu.CompilerParams(
            collective_id=0, has_side_effects=True, vmem_limit_bytes=56 * 1024 * 1024
        ),
    )(
        queries, keys_values, sink_logits, moe_rows, norm_gain.reshape(1, width),
        group_choice.reshape(1, tokens), member_choice.T, route_weight.T, w_gate, w_up, w_down,
    )


def solution(mesh):
    in_specs = (
        P(("ep", "tp"), None),
        P(None, ("ep", "tp"), None),
        P(),
        P("ep", None),
        P(),
        P("ep"),
        P("ep", None),
        P("ep", None),
        P("ep", None, "tp"),
        P("ep", None, "tp"),
        P("ep", None, "tp"),
    )
    out_specs = (P(("ep", "tp"), None), P("ep", "tp"))
    return jax.shard_map(shards, mesh=mesh, in_specs=in_specs, out_specs=out_specs, check_vma=False)
```

time: 81.2 us -> 66.6 us (0.82)
  the two profiles are of different devices: /device:TPU:18 before, /device:TPU:0 now
where the time goes in v1:
time: 66.6 us; the launch traced here: 66.4 us
  Pallas kernels  64.1 us (96%)
  local copies, waits for them, and re-layouts  1.58 us (2%)
    pallas_call x1, Pallas kernels, shards(): pl.pallas_call(functools.partial(kernel, n, tp, cap), out_shape=(pltpu.VM...  64.1 us
    unnamed x2, local copies, waits for them, and re-layouts  1.58 us

profile of v1, /device:TPU:0, one launch (start us, length us, event | category | flops | bytes accessed | tf_op | source)
XLA Modules:
  0.0 66.4 jit_solution(17668075887439420555)
XLA Ops:
  0.6 64.1 %shard_map.122 = (bf16[384,1024]{1,0:T(8,128)(2,1)S(1)}, bf16[256,512]{1,0:T(8,128)(2,1)S(1)}) custom-call(bf16[384,1024]{1,0:T(8,128)(2,1)} %q_hbm.1, bf16[2,384,256]{2,1,0:T(8,128)(2,1)} %kv_hbm.1, f32[16]{0:T(128)} %sink_ref.1, bf16[256,2048]{1,0:T(8,128)(2,1)} %rows_hbm.1, f32[1,2048]{1,0:T(1,128)} %bitcast.4, s32[1,256]{1,0:T(1,128)} %bitcast.7, ...), custom_call_target="tpu_custom_call" | custom-call | tf_op jit(solution)/shard_map/pallas_call | solution.py:472
  64.8 0.9 %copy.15 = bf16[384,1024]{1,0:T(8,128)(2,1)} copy(bf16[384,1024]{1,0:T(8,128)(2,1)S(1)} %get-tuple-element.2) | data formatting | bytes 1572864
  65.7 0.7 %copy.16 = bf16[256,512]{1,0:T(8,128)(2,1)} copy(bf16[256,512]{1,0:T(8,128)(2,1)S(1)} %get-tuple-element.3) | data formatting | bytes 524288

commit v2 on v1

--- a/solution.py
+++ b/solution.py
@@ -14,6 +14,7 @@
 EPG = 4
 TOP = 2
 CORES = 2
+ROW_PARTS = 4
 WIDE = 4
 RAWAT = 2
 LAG = 6
@@ -24,11 +25,11 @@
 
 def kernel(
     n, tp, cap,
-    q_hbm, kv_hbm, sink_ref, rows_hbm, gain_ref, group_ref, member_ref, rw_ref,
+    q_hbm, kv_hbm, sink_hbm, rows_hbm, gain_hbm, group_hbm, member_hbm, rw_hbm,
     wg_hbm, wu_hbm, wd_hbm,
     att_ref, mix_ref,
-    wg, wu, wd, q, rows, kvj, nrm, raw, posm, S, SN, X, H, O, R, acc, line, col,
-    loc, edge_s, edge_r, raw_s, raw_r, pos_s, pos_r, s_s, r1, x_s, x2, x3, h_s, h2, h3, o_s, o_r,
+    wg, wu, wd, q, rows, sink_ref, gain_ref, group_ref, member_ref, rw_ref, kvj, nrm, raw, posm, S, SN, X, H, O, R, acc, line, col,
+    small, loc, edge_s, edge_r, raw_s, raw_r, pos_s, pos_r, s_s, r1, x_s, x2, x3, h_s, h2, h3, o_s, o_r,
 ):
     e = lax.axis_index("ep")
     t = lax.axis_index("tp")
@@ -79,16 +80,32 @@
             barrier, inc=1, device_id=(lin2 // tp, lax.rem(lin2, tp)), device_id_type=MESH
         )
 
+    part = tokens // ROW_PARTS
+
+    def row_load(k):
+        at = pl.ds(k * part, part)
+        return pltpu.make_async_copy(rows_hbm.at[at], rows.at[at], loc.at[k])
+
+    row_loads = [row_load(k) for k in range(ROW_PARTS)]
     loads = [
-        pltpu.make_async_copy(rows_hbm, rows, loc.at[0]),
-        pltpu.make_async_copy(wg_hbm.at[0], wg, loc.at[1]),
-        pltpu.make_async_copy(wu_hbm.at[0], wu, loc.at[2]),
-        pltpu.make_async_copy(q_hbm, q, loc.at[3]),
-        pltpu.make_async_copy(kv_hbm, kvj.at[:, pl.ds(WINDOW, length)], loc.at[4]),
-        pltpu.make_async_copy(wd_hbm.at[0], wd, loc.at[5]),
+        pltpu.make_async_copy(wg_hbm.at[0], wg, loc.at[ROW_PARTS + 0]),
+        pltpu.make_async_copy(wu_hbm.at[0], wu, loc.at[ROW_PARTS + 1]),
+        pltpu.make_async_copy(q_hbm, q, loc.at[ROW_PARTS + 2]),
+        pltpu.make_async_copy(kv_hbm, kvj.at[:, pl.ds(WINDOW, length)], loc.at[ROW_PARTS + 3]),
+        pltpu.make_async_copy(wd_hbm.at[0], wd, loc.at[ROW_PARTS + 4]),
     ]
-    loads[0].start()
-
+    details = [
+        pltpu.make_async_copy(a, b, small.at[i])
+        for i, (a, b) in enumerate([
+            (group_hbm, group_ref), (member_hbm, member_ref), (rw_hbm, rw_ref),
+            (gain_hbm, gain_ref), (sink_hbm, sink_ref),
+        ])
+    ]
+    for c in details[:3] + row_loads + details[3:]:
+        c.start()
+
+    for c in details[:3]:
+        c.wait()
     a_i = lax.broadcasted_iota(jnp.int32, (tokens, tokens), 0)
     b_i = lax.broadcasted_iota(jnp.int32, (tokens, tokens), 1)
     erow = lax.broadcasted_iota(jnp.int32, (n, tokens), 0)
@@ -122,11 +139,14 @@
             nrm[block_of(k), at, :] = nv[:, k * dc : (k + 1) * dc]
         return 0
 
-    loads[0].wait()
-    for c in loads[1:]:
-        c.start()
-    with jax.named_scope("norm"):
-        lax.fori_loop(0, tokens // chunk, norm_rows, 0)
+    details[3].wait()
+    for k in range(ROW_PARTS):
+        row_loads[k].wait()
+        if k == ROW_PARTS - 1:
+            for c in loads:
+                c.start()
+        with jax.named_scope("norm"):
+            lax.fori_loop(k * part // chunk, (k + 1) * part // chunk, norm_rows, 0, unroll=2)
 
     def slots_of(side, x):
         slot = lax.broadcasted_iota(jnp.int32, (cap, tokens), 0)
@@ -272,15 +292,19 @@
     blocks = length // WINDOW
     units = 2 * blocks
 
+    def pass_on(g, r):
+        m = g * near + r
+        S[m] = gathered(slots_of(g, partner(r)), raw[g])
+        send_rows(m)
+
     def take_raw(g):
         m = g * near
         with jax.named_scope("w_raw"):
             expect(posm.at[g], pos_r.at[g])
             expect(raw.at[g], raw_r.at[g])
         with jax.named_scope("relay_rows"):
-            for r in range(1, near):
-                S[m + r] = gathered(slots_of(g, partner(r)), raw[g])
-                send_rows(m + r)
+            for r in range(1, near - 1):
+                pass_on(g, r)
             X[m, own] = gathered(slots_of(g, e), raw[g])
             spread(X, m, x_s, x2)
 
@@ -308,8 +332,8 @@
                 expect(X.at[m, pl.ds(0, ny)], r1.at[m])
             relay(X, m, x_s, x3)
 
+    loads[0].wait()
     loads[1].wait()
-    loads[2].wait()
 
     def when_raw(i, mark):
         for g in range(1, sides):
@@ -319,88 +343,109 @@
 
     early = lax.rem(e // (near // 2), 2) == lax.rem(e // near, 2)
 
+    def unit(u, _):
+        for half in range(2):
+            @pl.when(lax.rem(u, 2) == half)
+            def _(half=half):
+                with jax.named_scope("attend"):
+                    attend(blocks - 1 - u // 2, half)
+        return 0
+
+    def share(j):
+        m = chosen(j)
+        with jax.named_scope("w_h2"):
+            expect(H.at[m, pl.ds(0, ny - 1)], h2.at[m])
+        relay(H, m, h_s, h3)
+
+    def compute(j, _):
+        m = chosen(j)
+
+        @pl.when(j == n - 1)
+        def _():
+            fill(j)
+
+        @pl.when(j > 0)
+        def _():
+            with jax.named_scope("w_x3"):
+                expect(X.at[m, pl.ds(0, ny)], x3.at[m])
+
+        with jax.named_scope("gate_up"):
+            gate_up(m)
+        spread(H, m, h_s, h2)
+        return 0
+
+    def finish(j, _):
+        m = chosen(j)
+        with jax.named_scope("w_h3"):
+            expect(H.at[m, pl.ds(0, ny)], h3.at[m])
+        with jax.named_scope("down"):
+            down(m)
+
+        @pl.when(j > 0)
+        def _():
+            pltpu.make_async_remote_copy(
+                src_ref=O.at[m], dst_ref=R.at[m], send_sem=o_s.at[m], recv_sem=o_r.at[m],
+                device_id=(partner(m), t), device_id_type=MESH,
+            ).start()
+
+        @pl.when(j == 0)
+        def _():
+            combine(m, O)
+
+        return 0
+
     def step(i, _):
         @pl.when(early)
         def _():
             when_raw(i, RAWAT)
 
-        @pl.when(i >= 3)
+        @pl.when(i >= near - 1)
         def _():
             take(i + 1)
 
-        @pl.when(i > 0)
+        for g in range(1, sides):
+            @pl.when(i == near * g - 1)
+            def _(g=g):
+                pass_on(g, near - 1)
+
+        @pl.when((i == near - 1) & jnp.logical_not(early))
+        def _():
+            share(i - 1)
+
+        @pl.when((i > 0) & (i < n - 1))
         def _():
             fill(i)
 
-        @pl.when((i >= 3) & (i < 3))
-        def _():
-            take(i + 1)
-
-        @pl.when(i < n)
-        def _():
-            m = chosen(i)
-
-            @pl.when(i > 0)
-            def _():
-                with jax.named_scope("w_x3"):
-                    expect(X.at[m, pl.ds(0, ny)], x3.at[m])
-
-            with jax.named_scope("gate_up"):
-                gate_up(m)
-            spread(H, m, h_s, h2)
-
-        @pl.when(i < 3)
-        def _():
-            take(i + 1)
+        lax.fori_loop(jnp.where(i > n - 2, n, i), jnp.where(i >= n - 2, n, i + 1), compute, 0)
 
         @pl.when(i == 0)
         def _():
-            loads[3].wait()
-            loads[4].wait()
-            loads[5].wait()
-
-        @pl.when(i == units - 2)
+            for c in loads[2:]:
+                c.wait()
+            details[4].wait()
+            lax.fori_loop(0, units - 2, unit, 0)
+
+        @pl.when(jnp.logical_not(early))
+        def _():
+            when_raw(i, RAWAT)
+
+        @pl.when((i == 0) | (i == 2) | ((i == near - 1) & early) | ((i >= near) & (i - 1 < n)))
+        def _():
+            share(jnp.where(i == 0, 0, i - 1))
+
+        lax.fori_loop(
+            jnp.where(i <= near, jnp.maximum(i - 2, 0), jnp.minimum(i - 1, n)),
+            jnp.where(i < near, i - 1, jnp.minimum(i, n)), finish, 0,
+        )
+
+        @pl.when(i == n)
         def _():
             @pl.when(lin > 0)
             def _():
                 with jax.named_scope("w_edge"):
                     edge.wait_recv()
 
-        @pl.when(jnp.logical_not(early))
-        def _():
-            when_raw(i, RAWAT)
-
-        @pl.when((i >= 1) & (i - 1 < n))
-        def _():
-            m = chosen(i - 1)
-            with jax.named_scope("w_h2"):
-                expect(H.at[m, pl.ds(0, ny - 1)], h2.at[m])
-            relay(H, m, h_s, h3)
-
-        for half in range(2):
-            @pl.when((i < units) & (lax.rem(i, 2) == half))
-            def _(half=half):
-                with jax.named_scope("attend"):
-                    attend(blocks - 1 - i // 2, half)
-
-        @pl.when((i >= 1) & (i - 1 < n))
-        def _():
-            m = chosen(i - 1)
-            with jax.named_scope("w_h3"):
-                expect(H.at[m, pl.ds(0, ny)], h3.at[m])
-            with jax.named_scope("down"):
-                down(m)
-
-            @pl.when(i > 1)
-            def _():
-                pltpu.make_async_remote_copy(
-                    src_ref=O.at[m], dst_ref=R.at[m], send_sem=o_s.at[m], recv_sem=o_r.at[m],
-                    device_id=(partner(m), t), device_id_type=MESH,
-                ).start()
-
-            @pl.when(i == 1)
-            def _():
-                combine(m, O)
+            lax.fori_loop(units - 2, units, unit, 0)
 
         @pl.when(i == 3)
         def _():
@@ -476,7 +521,7 @@
             pltpu.VMEM((tokens, out), BF16),
         ),
         in_specs=[
-            anyspace, anyspace, pl.BlockSpec(memory_space=pltpu.SMEM), anyspace, vmem, vmem, vmem, vmem,
+            anyspace, anyspace, anyspace, anyspace, anyspace, anyspace, anyspace, anyspace,
             anyspace, anyspace, anyspace,
         ],
         out_specs=(vmem, vmem),
@@ -486,6 +531,11 @@
             pltpu.VMEM((ff, out), BF16),
             pltpu.VMEM(queries.shape, BF16),
             pltpu.VMEM(moe_rows.shape, BF16),
+            pltpu.SMEM(sink_logits.shape, F32),
+            pltpu.VMEM((1, width), F32),
+            pltpu.VMEM((1, tokens), jnp.int32),
+            pltpu.VMEM((TOP, tokens), jnp.int32),
+            pltpu.VMEM((TOP, tokens), F32),
             pltpu.VMEM((2, WINDOW + length, keys_values.shape[2]), BF16),
             pltpu.VMEM((tp, tokens, width // tp), BF16),
             pltpu.VMEM((n // min(EPG, n), tokens, width // tp), BF16),
@@ -499,7 +549,7 @@
             pltpu.VMEM((tokens, out), F32),
             pltpu.VMEM((128, tokens), F32),
             pltpu.VMEM((tokens, 128), F32),
-            dma((6,)), dma, dma,
+            dma((5,)), dma((5 + ROW_PARTS,)), dma, dma,
             dma((n // min(EPG, n),)), dma((n // min(EPG, n),)), dma((n // min(EPG, n),)), dma((n // min(EPG, n),)),
             dma((n,)), dma((n,)), dma((n,)), dma((n,)), dma((n,)),
             dma((n,)), dma((n,)), dma((n,)), dma((n,)), dma((n,)),

time: 66.6 us -> 63.9 us (0.959); the launches traced: 66.4 us -> 62.6 us
  Pallas kernels: 64.1 us -> 60.4 us
    pallas_call x1, Pallas kernels: 64.1 us -> 60.4 us  [shards(): pl.pallas_call(functools.partial(kernel, n, tp, cap), out_shape=(pltpu.VM...]
where the time goes in v2:
time: 63.9 us; the launch traced here: 62.6 us
  Pallas kernels  60.4 us (95%)
  local copies, waits for them, and re-layouts  1.58 us (2%)
  between operations  0.64 us (1%)
    pallas_call x1, Pallas kernels, shards(): pl.pallas_call(functools.partial(kernel, n, tp, cap), out_shape=(pltpu.VM...  60.4 us
    unnamed x2, local copies, waits for them, and re-layouts  1.58 us

profile of v2, /device:TPU:0, one launch (start us, length us, event | category | flops | bytes accessed | tf_op | source)
XLA Modules:
  0.0 62.6 jit_solution(208790360313796276)
XLA Ops:
  0.6 60.4 %shard_map.122 = (bf16[384,1024]{1,0:T(8,128)(2,1)S(1)}, bf16[256,512]{1,0:T(8,128)(2,1)S(1)}) custom-call(bf16[384,1024]{1,0:T(8,128)(2,1)} %q_hbm.1, bf16[2,384,256]{2,1,0:T(8,128)(2,1)} %kv_hbm.1, f32[16]{0:T(128)} %sink_hbm.1, bf16[256,2048]{1,0:T(8,128)(2,1)} %rows_hbm.1, f32[1,2048]{1,0:T(1,128)} %bitcast.4, s32[1,256]{1,0:T(1,128)} %bitcast.7, ...), custom_call_target="tpu_custom_call" | custom-call | tf_op jit(solution)/shard_map/pallas_call | solution.py:517
  61.0 0.9 %copy.15 = bf16[384,1024]{1,0:T(8,128)(2,1)} copy(bf16[384,1024]{1,0:T(8,128)(2,1)S(1)} %get-tuple-element.2) | data formatting | bytes 1572864
  61.9 0.7 %copy.16 = bf16[256,512]{1,0:T(8,128)(2,1)} copy(bf16[256,512]{1,0:T(8,128)(2,1)S(1)} %get-tuple-element.3) | data formatting | bytes 524288

commit v3 on v2

--- a/solution.py
+++ b/solution.py
@@ -71,13 +71,16 @@
         pl.semaphore_signal(barrier, inc=1, device_id=(partner(m), t), device_id_type=MESH)
         return 0
 
-    lax.fori_loop(1, n, greet, 0)
+    lax.fori_loop(1, near, greet, 0)
+    lax.fori_loop(1, sides, lambda g, _: greet(g * near, _), 0)
     for j in range(1, ny):
         pl.semaphore_signal(barrier, inc=1, device_id=(e, ypeer(j)), device_id_type=MESH)
     pl.semaphore_signal(barrier, inc=1, device_id=(e, mate), device_id_type=MESH)
-    for lin2 in (after, before):
+
+    @pl.when(lin > 0)
+    def _():
         pl.semaphore_signal(
-            barrier, inc=1, device_id=(lin2 // tp, lax.rem(lin2, tp)), device_id_type=MESH
+            barrier, inc=1, device_id=(before // tp, lax.rem(before, tp)), device_id_type=MESH
         )
 
     part = tokens // ROW_PARTS
@@ -193,7 +196,8 @@
         return 0
 
     with jax.named_scope("barrier"):
-        pl.semaphore_wait(barrier, (n - 1) + (ny - 1) + 1 + 2)
+        greeted = (near - 1) + (sides - 1) + (ny - 1) + 1
+        pl.semaphore_wait(barrier, jnp.where(lin < total - 1, greeted + 1, greeted))
     with jax.named_scope("build"):
         first_near = near // 2
         send_near(first_near)
@@ -341,7 +345,7 @@
             def _(g=g):
                 take_raw(g)
 
-    early = lax.rem(e // (near // 2), 2) == lax.rem(e // near, 2)
+    early = lin >= 0
 
     def unit(u, _):
         for half in range(2):
@@ -416,7 +420,7 @@
         def _():
             fill(i)
 
-        lax.fori_loop(jnp.where(i > n - 2, n, i), jnp.where(i >= n - 2, n, i + 1), compute, 0)
+        lax.fori_loop(i, jnp.where(i > n - 2, i, i + 1), compute, 0)
 
         @pl.when(i == 0)
         def _():
@@ -429,12 +433,18 @@
         def _():
             when_raw(i, RAWAT)
 
+        @pl.when(i == near)
+        def _():
+            finish(i - 2, 0)
+
         @pl.when((i == 0) | (i == 2) | ((i == near - 1) & early) | ((i >= near) & (i - 1 < n)))
         def _():
             share(jnp.where(i == 0, 0, i - 1))
 
+        lax.fori_loop(jnp.where(i == n - 2, n - 1, n), n, compute, 0)
+
         lax.fori_loop(
-            jnp.where(i <= near, jnp.maximum(i - 2, 0), jnp.minimum(i - 1, n)),
+            jnp.where(i < near, jnp.maximum(i - 2, 0), jnp.minimum(i - 1, n)),
             jnp.where(i < near, i - 1, jnp.minimum(i, n)), finish, 0,
         )
 

time: 63.9 us -> 63.4 us (level); the launches traced: 62.6 us -> 63.2 us
  no operation moved by 1% of the time
where the time goes in v3:
time: 63.4 us; the launch traced here: 63.2 us
  Pallas kernels  61 us (96%)
  local copies, waits for them, and re-layouts  1.58 us (2%)
  between operations  0.64 us (1%)
    pallas_call x1, Pallas kernels, shards(): pl.pallas_call(functools.partial(kernel, n, tp, cap), out_shape=(pltpu.VM...  61 us
    unnamed x2, local copies, waits for them, and re-layouts  1.58 us

profile of v3, /device:TPU:0, one launch (start us, length us, event | category | flops | bytes accessed | tf_op | source)
XLA Modules:
  0.0 63.2 jit_solution(13108828336110015165)
XLA Ops:
  0.6 61.0 %shard_map.122 = (bf16[384,1024]{1,0:T(8,128)(2,1)S(1)}, bf16[256,512]{1,0:T(8,128)(2,1)S(1)}) custom-call(bf16[384,1024]{1,0:T(8,128)(2,1)} %q_hbm.1, bf16[2,384,256]{2,1,0:T(8,128)(2,1)} %kv_hbm.1, f32[16]{0:T(128)} %sink_hbm.1, bf16[256,2048]{1,0:T(8,128)(2,1)} %rows_hbm.1, f32[1,2048]{1,0:T(1,128)} %bitcast.4, s32[1,256]{1,0:T(1,128)} %bitcast.7, ...), custom_call_target="tpu_custom_call" | custom-call | tf_op jit(solution)/shard_map/pallas_call | solution.py:527
  61.6 0.9 %copy.15 = bf16[384,1024]{1,0:T(8,128)(2,1)} copy(bf16[384,1024]{1,0:T(8,128)(2,1)S(1)} %get-tuple-element.2) | data formatting | bytes 1572864
  62.5 0.7 %copy.16 = bf16[256,512]{1,0:T(8,128)(2,1)} copy(bf16[256,512]{1,0:T(8,128)(2,1)S(1)} %get-tuple-element.3) | data formatting | bytes 524288
